TPU v7x, 32 devices: a whole 2x2x4 slice. The times are simulated.
32 devices in a mesh: sp: 8 (over z, y), dp: 4 (over x, core).
Axes of the slice: x: 2, y: 2, z: 4, core: 2. Of those that a mesh axis runs over, the one named last changes fastest.
Arguments:
- query_nope: bfloat16 [4, 2048, 16, 128], P('dp', 'sp'), may hold values from -6 to 6
- query_rope: bfloat16 [4, 2048, 16, 64], P('dp', 'sp'), may hold values from -160 to 160
- latent: bfloat16 [4, 2048, 256], P('dp', 'sp'), may hold values from -6 to 6
- key_rope: bfloat16 [4, 2048, 64], P('dp', 'sp'), may hold values from -4 to 4
- resid: bfloat16 [4, 2048, 2048], P('dp', 'sp'), may hold values from -6 to 6
- latent_gain: float32 [256], replicated, may hold values from 0.1 to 1.9
- key_up: bfloat16 [256, 2048], P(None, 'sp'), may hold values from -0.375 to 0.375
- value_up: bfloat16 [256, 2048], P(None, 'sp'), may hold values from -0.375 to 0.375
- out_proj: bfloat16 [2048, 2048], P('sp', 'dp'), may hold values from -0.125 to 0.125
- norm_gain: float32 [2048], replicated, may hold values from 0.1 to 1.9
- expert_gate: bfloat16 [8, 2048, 1024], P('sp'), may hold values from -0.125 to 0.125
- expert_up: bfloat16 [8, 2048, 1024], P('sp'), may hold values from -0.125 to 0.125
- expert_down: bfloat16 [8, 1024, 2048], P('sp'), may hold values from -0.1875 to 0.1875
- routes: int32 [4, 2048, 2], P('dp', 'sp'), may hold values from 0 to 7, all different within a row; in each aligned block of 256 rows (0 to 255, 256 to 511, ..., all dimensions but the last counted through in order) at most 128 rows name the same one
- route_weight: float32 [4, 2048, 2], P('dp', 'sp'), may hold values from 0.2 to 1
Outputs:
- mixed: bfloat16 [4, 2048, 2048], P('dp', 'sp')
Inputs may be any that keep to these rules, and one draw needn't show every extreme that they name: `routes`: each token names two different experts. Among the tokens of one device no expert is named more than 128 times, and in every draw some expert is named exactly 128 times by some device's tokens.
All inputs are finite; a program needn't handle non-finite values.
Results may differ from a plain program's by a relative error of at most 0.0075.
Values may be sent and summed in bfloat16 or wider, within the bound.
No kernel may reach another device: no remote copies, remote signals or barrier semaphores. Data moves between devices by JAX's collectives and lax.ppermute only.
A program may use at most 128 MiB of HBM per device.

v0:
```python
import jax
import jax.numpy as jnp
from jax import lax
from jax.sharding import PartitionSpec as P

epsilon = 1e-06
rope_base = 10000.0
masked_score = -1e30


def rotate(values, positions):
    half_width = values.shape[-1] // 2
    frequency = rope_base ** (-jnp.arange(half_width, dtype=jnp.float32) / half_width)
    angles = positions.astype(jnp.float32)[:, None] * frequency[None, :]
    cosine = jnp.cos(angles)
    sine_part = jnp.sin(angles)
    if values.ndim == 3:
        cosine = cosine[:, None, :]
        sine_part = sine_part[:, None, :]
    floats = values.astype(jnp.float32)
    first_half = floats[..., :half_width]
    second_half = floats[..., half_width:]
    turned = jnp.concatenate(
        [
            first_half * cosine - second_half * sine_part,
            second_half * cosine + first_half * sine_part,
        ],
        axis=-1,
    )
    return turned.astype(jnp.bfloat16)


def rms_scaled(values, gain):
    floats = values.astype(jnp.float32)
    return floats * lax.rsqrt(jnp.mean(floats * floats, axis=-1, keepdims=True) + epsilon) * gain


def assign_slots(route_block, experts_all, capacity):
    flat_routes = route_block.reshape(-1)
    onehot = (flat_routes[:, None] == jnp.arange(experts_all, dtype=jnp.int32)[None, :]).astype(
        jnp.int32
    )
    earlier = jnp.cumsum(onehot, axis=0) - onehot
    placed = jnp.sum(earlier * onehot, axis=1)
    return flat_routes * capacity + placed


def fill_slots(rows, slot_ids, experts_all, capacity):
    pairs = slot_ids.shape[0]
    matches = jnp.arange(experts_all * capacity, dtype=jnp.int32)[:, None] == slot_ids[None, :]
    source = (
        jnp.sum(jnp.where(matches, jnp.arange(pairs, dtype=jnp.int32)[None, :], 0), axis=1) // 2
    )
    filled = jnp.any(matches, axis=1)
    picked = jnp.take(rows, source, axis=0)
    chosen = jnp.where(filled[:, None], picked, jnp.zeros_like(picked))
    return chosen.reshape(experts_all, capacity, rows.shape[-1])


def combine_slots(returned, slot_ids, weights):
    flat_back = returned.reshape(-1, returned.shape[-1])
    picked = (
        jnp.take(flat_back, slot_ids, axis=0).astype(jnp.float32).reshape(weights.shape[0], 2, -1)
    )
    return jnp.sum(weights[:, :, None] * picked, axis=1)


def shards(
    query_nope,
    query_rope,
    latent,
    key_rope,
    resid,
    latent_gain,
    key_up,
    value_up,
    out_proj,
    norm_gain,
    expert_gate,
    expert_up,
    expert_down,
    routes,
    route_weight,
):
    tokens_here = latent.shape[1]
    sp_count = lax.axis_size("sp")
    length = tokens_here * sp_count
    block = min(512, length)
    blocks = length // block
    local_pos = lax.axis_index("sp") * tokens_here + jnp.arange(tokens_here, dtype=jnp.int32)
    latent_normed = rms_scaled(latent[0], latent_gain).astype(jnp.bfloat16)
    key_turned = rotate(key_rope[0], local_pos)
    query_turned = rotate(query_rope[0], local_pos)
    all_latent, all_keyturn = (
        lax.all_gather(latent_normed, "sp", axis=0, tiled=True),
        lax.all_gather(key_turned, "sp", axis=0, tiled=True),
    )
    query_plain, query_turn = (
        lax.all_to_all(query_nope[0], "sp", split_axis=1, concat_axis=0, tiled=True),
        lax.all_to_all(query_turned, "sp", split_axis=1, concat_axis=0, tiled=True),
    )
    heads_here = query_plain.shape[1]
    key_plain = (
        jnp.dot(all_latent, key_up, preferred_element_type=jnp.float32)
        .astype(jnp.bfloat16)
        .reshape(length, heads_here, -1)
    )
    value_heads = (
        jnp.dot(all_latent, value_up, preferred_element_type=jnp.float32)
        .astype(jnp.bfloat16)
        .reshape(length, heads_here, -1)
    )
    scale = (query_plain.shape[-1] + query_turn.shape[-1]) ** (-0.5)
    key_ids = jnp.arange(length, dtype=jnp.int32)

    def one_block(items):
        index, plain_block, turn_block = items
        scores = jnp.einsum(
            "bhd,shd->hbs", plain_block, key_plain, preferred_element_type=jnp.float32
        )
        scores = (
            scores
            + jnp.einsum("bhr,sr->hbs", turn_block, all_keyturn, preferred_element_type=jnp.float32)
        ) * scale
        row_ids = index * block + jnp.arange(block, dtype=jnp.int32)
        allowed = key_ids[None, :] <= row_ids[:, None]
        scores = jnp.where(allowed[None], scores, masked_score)
        largest = jnp.max(scores, axis=-1, keepdims=True)
        powers = jnp.exp(scores - largest)
        attend = (powers / jnp.sum(powers, axis=-1, keepdims=True)).astype(jnp.bfloat16)
        return jnp.einsum(
            "hbs,shd->bhd", attend, value_heads, preferred_element_type=jnp.float32
        ).astype(jnp.bfloat16)

    attended = lax.map(
        one_block,
        (
            jnp.arange(blocks, dtype=jnp.int32),
            query_plain.reshape(blocks, block, heads_here, -1),
            query_turn.reshape(blocks, block, heads_here, -1),
        ),
    )
    attended = attended.reshape(length, heads_here, -1)
    token_heads = lax.all_to_all(attended, "sp", split_axis=0, concat_axis=1, tiled=True)
    flat_heads = token_heads.reshape(tokens_here, -1)
    head_rows = lax.all_gather(out_proj, "dp", axis=1, tiled=True)
    projected = jnp.dot(
        flat_heads,
        lax.all_gather(head_rows, "sp", axis=0, tiled=True),
        preferred_element_type=jnp.float32,
    ).astype(jnp.bfloat16)
    after_attention = resid[0].astype(jnp.float32) + projected.astype(jnp.float32)
    normed = rms_scaled(after_attention, norm_gain).astype(jnp.bfloat16)
    experts_all = sp_count * expert_gate.shape[0]
    capacity = 4 * tokens_here // experts_all
    slot_ids = assign_slots(routes[0], experts_all, capacity)
    outgoing = fill_slots(normed, slot_ids, experts_all, capacity)
    arrived = lax.all_to_all(outgoing, "sp", split_axis=0, concat_axis=0, tiled=True)
    senders, slots_now, width = arrived.shape
    rows = arrived.reshape(senders * slots_now, width)
    gate = jnp.dot(rows, expert_gate[0], preferred_element_type=jnp.float32)
    upward = jnp.dot(rows, expert_up[0], preferred_element_type=jnp.float32)
    hidden = (jax.nn.silu(gate) * upward).astype(jnp.bfloat16)
    result = jnp.dot(hidden, expert_down[0], preferred_element_type=jnp.float32).astype(
        jnp.bfloat16
    )
    returned = lax.all_to_all(
        result.reshape(senders, slots_now, width), "sp", split_axis=0, concat_axis=0, tiled=True
    )
    routed = combine_slots(returned, slot_ids, route_weight[0])
    return (after_attention + routed).astype(jnp.bfloat16)[None]


def solution(mesh):
    return jax.shard_map(
        shards,
        mesh=mesh,
        in_specs=(
            P("dp", "sp", None, None),
            P("dp", "sp", None, None),
            P("dp", "sp", None),
            P("dp", "sp", None),
            P("dp", "sp", None),
            P(),
            P(None, "sp"),
            P(None, "sp"),
            P("sp", "dp"),
            P(),
            P("sp", None, None),
            P("sp", None, None),
            P("sp", None, None),
            P("dp", "sp", None),
            P("dp", "sp", None),
        ),
        out_specs=P("dp", "sp", None),
        check_vma=False,
    )
```

profile of v0, /device:TPU:0, one launch (start us, length us, event | category | flops | bytes accessed | tf_op | source)
XLA Modules:
  0.0 489.6 jit_solution(9054582442500225814)
XLA Ops:
  12.2 16.1 %all-gather.6.cloned.1.call-done = bf16[256,2048]{1,0:T(8,128)(2,1)} async-done(((bf16[256,512]{1,0:T(8,128)(2,1)}), bf16[256,2048]{1,0:T(8,128)(2,1)}) %all-gather.6.cloned.1.call-update) | async-done | bytes 1048592 | tf_op jit(solution)/shard_map/all_gather | solution.py:146
  29.4 5.5 %all-to-all-start.1 = ((bf16[256,16,64]{0,2,1:T(8,128)(2,1)}), bf16[256,16,64]{0,2,1:T(8,128)(2,1)S(1)}, u32[]{:S(2)}, u32[]{:S(2)}) async-start(bf16[256,16,64]{0,2,1:T(8,128)(2,1)} %pad_maximum_fusion), calls=%async_computation.1 | async-start | bytes 1048576 | tf_op jit(solution)/shard_map/all_to_all | solution.py:100
  36.2 17.7 %all-to-all-done.1 = bf16[256,16,64]{0,2,1:T(8,128)(2,1)S(1)} async-done(((bf16[256,16,64]{0,2,1:T(8,128)(2,1)}), bf16[256,16,64]{0,2,1:T(8,128)(2,1)S(1)}, u32[]{:S(2)}, u32[]{:S(2)}) %all-to-all-start.1) | async-done | bytes 524320 | tf_op jit(solution)/shard_map/all_to_all | solution.py:100
  54.0 3.6 all-to-all-start
  57.6 55.9 %all_gather.13 = bf16[2048,64]{0,1:T(8,128)(2,1)S(1)} all-gather(bf16[256,64]{0,1:T(8,128)(2,1)S(1)} %pad_maximum_fusion.1), channel_id=1, replica_groups=mesh['sp'=8,'dp'=4] {'sp'}, dimensions={0}, use_global_device_ids=true | all-gather | bytes 294912 | tf_op jit(solution)/shard_map/all_gather | solution.py:96
  115.1 2.8 convolution_convert_fusion.1
  119.5 2.4 convolution_convert_fusion
  121.9 2.3 copy.93
  124.3 73.1 %while.11 = (s32[]{:T(128)}, bf16[4,512,2,128]{3,1,0,2:T(8,128)(2,1)}, s32[4]{0:T(128)S(1)}, bf16[4,512,2,128]{3,1,0,2:T(8,128)(2,1)S(1)}, bf16[2048,2,128]{2,0,...) while((s32[]{:T(128)}, ...), condition=%wide.region_4.5_spmd.clone, body=%wide.region_1.4_spmd.clone.sunk | while | flops 1360139776 | bytes 93205688 | solution.py:135
  127.3 2.8 fusion.75
  133.3 9.1 %fusion.77 = bf16[4,512,2,128]{3,1,0,2:T(8,128)(2,1)} fusion(bf16[4,512,2,128]{3,1,0,2:T(8,128)(2,1)} %get-tuple-element.211, s32[]{:T(128)} %get-tuple-element.210, bf16[2048,2,128]{2,0,1:T(8,128)(2,1)S(1)} %copy-done.5, f32[2,512]{1,0:T(2,128)S(1)} %fusion.76, f32[2,512,2048]{2,1,0:T(8,128)} %copy-done.2), kind=kOutput, calls=%fused_computation.13.clone.1 | convolution fusion | flops 543296512 | bytes 18092544 | tf_op jit(solution)/shard_map/while/body/eval_jaxpr/hbs,shd->bhd/dot_general | solution.py:131
  145.5 2.8 fusion.75
  151.5 9.2 %fusion.77 = bf16[4,512,2,128]{3,1,0,2:T(8,128)(2,1)} fusion(bf16[4,512,2,128]{3,1,0,2:T(8,128)(2,1)} %get-tuple-element.211, s32[]{:T(128)} %get-tuple-element.210, bf16[2048,2,128]{2,0,1:T(8,128)(2,1)S(1)} %copy-done.5, f32[2,512]{1,0:T(2,128)S(1)} %fusion.76, f32[2,512,2048]{2,1,0:T(8,128)} %copy-done.2), kind=kOutput, calls=%fused_computation.13.clone.1 | convolution fusion | flops 543296512 | bytes 18092544 | tf_op jit(solution)/shard_map/while/body/eval_jaxpr/hbs,shd->bhd/dot_general | solution.py:131
  163.8 2.8 fusion.75
  169.8 9.1 %fusion.77 = bf16[4,512,2,128]{3,1,0,2:T(8,128)(2,1)} fusion(bf16[4,512,2,128]{3,1,0,2:T(8,128)(2,1)} %get-tuple-element.211, s32[]{:T(128)} %get-tuple-element.210, bf16[2048,2,128]{2,0,1:T(8,128)(2,1)S(1)} %copy-done.5, f32[2,512]{1,0:T(2,128)S(1)} %fusion.76, f32[2,512,2048]{2,1,0:T(8,128)} %copy-done.2), kind=kOutput, calls=%fused_computation.13.clone.1 | convolution fusion | flops 543296512 | bytes 18092544 | tf_op jit(solution)/shard_map/while/body/eval_jaxpr/hbs,shd->bhd/dot_general | solution.py:131
  181.9 2.8 fusion.75
  188.0 9.4 %fusion.77 = bf16[4,512,2,128]{3,1,0,2:T(8,128)(2,1)} fusion(bf16[4,512,2,128]{3,1,0,2:T(8,128)(2,1)} %get-tuple-element.211, s32[]{:T(128)} %get-tuple-element.210, bf16[2048,2,128]{2,0,1:T(8,128)(2,1)S(1)} %copy-done.5, f32[2,512]{1,0:T(2,128)S(1)} %fusion.76, f32[2,512,2048]{2,1,0:T(8,128)} %copy-done.2), kind=kOutput, calls=%fused_computation.13.clone.1 | convolution fusion | flops 543296512 | bytes 18092544 | tf_op jit(solution)/shard_map/while/body/eval_jaxpr/hbs,shd->bhd/dot_general | solution.py:131
  197.3 3.7 copy.95
  201.0 3.7 all-to-all-start.2
  207.4 28.0 %all-to-all-done.2 = bf16[2048,2,128]{2,1,0:T(2,128)(2,1)S(1)} async-done(((bf16[2048,2,128]{2,1,0:T(2,128)(2,1)}), bf16[2048,2,128]{2,1,0:T(2,128)(2,1)S(1)}, u32[]{:S(2)}, u32[]{:S(2)}) %all-to-all-start.2) | async-done | bytes 1048608 | tf_op jit(solution)/shard_map/all_to_all | solution.py:144
  236.2 6.1 %multiply_reduce_fusion.1 = (f32[256]{0:T(256)S(1)}, f32[256,2048]{1,0:T(8,128)S(1)}) fusion(bf16[256,2048]{0,1:T(8,128)(2,1)S(1)} %bitcast.150, bf16[2048,2048]{1,0:T(8,128)(2,1)} %all-gather.8.cloned.1.call-done, bf16[1,256,2048]{2,1,0:T(8,128)(2,1)} %param.21), kind=kOutput, calls=%fused_computation.42 | convolution fusion | flops 2150629120 | bytes 12583936 | tf_op jit(solution)/shard_map/dot_general | solution.py:147
  242.5 6.0 %gather_fusion = bf16[1024,2048]{1,0:T(8,128)(2,1)} fusion(bf16[256,2048]{1,0:T(8,128)(2,1)S(1)} %multiply_convert_fusion.1, s32[1024]{0:T(1024)S(1)} %broadcast_clamp_fusion), kind=kCustom, calls=%fused_computation | custom fusion | bytes 8392704 | tf_op jit(solution)/shard_map/jit(_take)/gather | solution.py:55
  248.5 2.6 select_select_fusion
  251.1 95.5 %all_to_all.55 = bf16[8,128,2048]{2,1,0:T(8,128)(2,1)S(1)} all-to-all(bf16[8,128,2048]{2,1,0:T(8,128)(2,1)S(1)} %select_select_fusion), channel_id=1, replica_groups=mesh['sp'=8,'dp'=4] {'sp'}, dimensions={0} | all-to-all | bytes 8388608 | tf_op jit(solution)/shard_map/all_to_all | solution.py:158
  346.6 4.5 fusion.20
  351.1 5.4 %multiply_convert_fusion = bf16[1024,1024]{1,0:T(8,128)(2,1)S(1)} fusion(f32[1024,1024]{1,0:T(8,128)S(1)} %fusion.20, bf16[1024,2048]{1,0:T(8,128)(2,1)S(1)} %bitcast.154, bf16[1,2048,1024]{2,1,0:T(8,128)(2,1)S(1)} %copy-done.10), kind=kOutput, calls=%fused_computation.31 | convolution fusion | flops 4301258752 | bytes 14680064 | tf_op jit(solution)/shard_map/dot_general | solution.py:161
  356.5 6.1 %fusion.24 = bf16[1024,2048]{1,0:T(8,128)(2,1)} fusion(bf16[1024,1024]{1,0:T(8,128)(2,1)S(1)} %multiply_convert_fusion, bf16[1,1024,2048]{2,1,0:T(8,128)(2,1)S(1)} %copy-done.11), kind=kOutput, calls=%fused_computation.34 | convolution fusion | flops 4297064448 | bytes 10485760 | tf_op jit(solution)/shard_map/dot_general | solution.py:164
  362.6 4.9 all-to-all-start.4
  368.4 91.0 %all-to-all-done.4 = bf16[8,128,2048]{2,1,0:T(8,128)(2,1)} async-done(((bf16[8,128,2048]{2,1,0:T(8,128)(2,1)}), bf16[8,128,2048]{2,1,0:T(8,128)(2,1)}, u32[]{:S(2)}, u32[]{:S(2)}) %all-to-all-start.4) | async-done | bytes 4194336 | tf_op jit(solution)/shard_map/all_to_all | solution.py:167
  459.4 8.0 %gather_fusion.1 = bf16[512,2048]{1,0:T(8,128)(2,1)} fusion(bf16[1024,2048]{1,0:T(8,128)(2,1)} %bitcast.33, s32[1024]{0:T(1024)S(1)} %pad_clamp_fusion), kind=kCustom, calls=%fused_computation.1 | custom fusion | bytes 4196352 | tf_op jit(solution)/shard_map/jit(_take)/gather | solution.py:63
  467.4 4.4 gather.15
  471.9 9.9 %multiply_reduce_fusion = f32[256,2048]{1,0:T(8,128)S(1)} fusion(bf16[256,2,2048]{2,1,0:T(2,128)(2,1)} %gather.15, pred[256,2]{1,0:T(8,128)(4,1)S(1)} %copy.102, f32[256,2]{1,0:T(8,128)S(1)} %copy.98), kind=kLoop, calls=%fused_computation.30 | loop fusion | flops 3670016 | bytes 4196864 | tf_op jit(solution)/shard_map/reduce_sum | solution.py:65
  (114 shorter events, 39.5 us)
Async XLA Ops:
  6.5 108.5 %copy-start = (bf16[256,256]{1,0:T(8,128)(2,1)S(1)}, bf16[256,256]{1,0:T(8,128)(2,1)}, u32[]{:S(2)}) copy-start(bf16[256,256]{1,0:T(8,128)(2,1)} %param.23) | copy-start | bytes 393220
  6.5 28.3 %copy-start.4 = (bf16[1,256,16,128]{3,2,1,0:T(8,128)(2,1)S(1)}, bf16[1,256,16,128]{3,2,1,0:T(8,128)(2,1)}, u32[]{:S(2)}) copy-start(bf16[1,256,16,128]{3,2,1,0:T(8,128)(2,1)} %param.17) | copy-start | bytes 3145732
  6.5 21.8 %all-gather.6.cloned.1.call-start = ((), (), s32[]{:S(2)}) async-start(), calls=%async_computation.6 | async-start | bytes 1310720 | tf_op jit(solution)/shard_map/all_gather | solution.py:146
  7.3 107.8 %all-gather.4.cloned.1.call-start = ((), (), s32[]{:S(2)}) async-start(), calls=%async_computation.5 | async-start | bytes 1179648 | tf_op jit(solution)/shard_map/all_gather | solution.py:95
  10.0 226.1 %all-gather.8.cloned.1.call-start = ((), (), s32[]{:S(2)}) async-start(), calls=%async_computation.7 | async-start | bytes 9437184 | tf_op jit(solution)/shard_map/all_gather | solution.py:149
  29.4 24.6 %all-to-all-start.1 = ((bf16[256,16,64]{0,2,1:T(8,128)(2,1)}), bf16[256,16,64]{0,2,1:T(8,128)(2,1)S(1)}, u32[]{:S(2)}, u32[]{:S(2)}) async-start(bf16[256,16,64]{0,2,1:T(8,128)(2,1)} %pad_maximum_fusion), calls=%async_computation.1 | async-start | bytes 1048576 | tf_op jit(solution)/shard_map/all_to_all | solution.py:100
  54.0 70.2 %all-to-all-start = ((bf16[256,16,128]{2,0,1:T(8,128)(2,1)}), bf16[256,16,128]{2,0,1:T(8,128)(2,1)S(1)}, u32[]{:S(2)}, u32[]{:S(2)}) async-start(bf16[256,16,128]{2,0,1:T(8,128)(2,1)} %bitcast.127), calls=%async_computation | async-start | bytes 2097152 | tf_op jit(solution)/shard_map/all_to_all | solution.py:99
  115.1 4.4 copy-start.3
  130.1 3.2 copy-start.2
  130.1 3.2 copy-start.5
  148.3 3.2 copy-start.2
  148.3 3.2 copy-start.5
  166.5 3.2 copy-start.2
  166.6 3.2 copy-start.5
  184.7 3.2 copy-start.2
  184.7 3.2 copy-start.5
  197.3 7.4 %copy-start.6 = (s32[1,256,2]{1,2,0:T(2,128)S(1)}, s32[1,256,2]{1,2,0:T(2,128)}, u32[]{:S(2)}) copy-start(s32[1,256,2]{1,2,0:T(2,128)} %param.30) | copy-start | bytes 6148
  201.0 34.4 %all-to-all-start.2 = ((bf16[2048,2,128]{2,1,0:T(2,128)(2,1)}), bf16[2048,2,128]{2,1,0:T(2,128)(2,1)S(1)}, u32[]{:S(2)}, u32[]{:S(2)}) async-start(bf16[2048,2,128]{2,1,0:T(2,128)(2,1)} %copy.95), calls=%async_computation.2 | async-start | bytes 2097152 | tf_op jit(solution)/shard_map/all_to_all | solution.py:144
  236.1 6.1 %copy-start.7 = (f32[2048]{0:T(1024)S(1)}, f32[2048]{0:T(1024)}, u32[]{:S(2)}) copy-start(f32[2048]{0:T(1024)} %param.26) | copy-start | bytes 24580
  251.1 95.5 %copy-start.9 = (bf16[1,2048,1024]{2,1,0:T(8,128)(2,1)S(1)}, bf16[1,2048,1024]{2,1,0:T(8,128)(2,1)}, u32[]{:S(2)}) copy-start(bf16[1,2048,1024]{2,1,0:T(8,128)(2,1)} %param.28) | copy-start | bytes 12582916
  346.6 4.5 copy-start.10
  351.1 5.4 %copy-start.11 = (bf16[1,1024,2048]{2,1,0:T(8,128)(2,1)S(1)}, bf16[1,1024,2048]{2,1,0:T(8,128)(2,1)}, u32[]{:S(2)}) copy-start(bf16[1,1024,2048]{2,1,0:T(8,128)(2,1)} %param.29) | copy-start | bytes 12582916
  362.6 5.6 %copy-start.8 = (f32[1,256,2]{1,2,0:T(2,128)S(1)}, f32[1,256,2]{1,2,0:T(2,128)}, u32[]{:S(2)}) copy-start(f32[1,256,2]{1,2,0:T(2,128)} %param.31) | copy-start | bytes 6148
  362.6 96.9 %all-to-all-start.4 = ((bf16[8,128,2048]{2,1,0:T(8,128)(2,1)}), bf16[8,128,2048]{2,1,0:T(8,128)(2,1)}, u32[]{:S(2)}, u32[]{:S(2)}) async-start(bf16[8,128,2048]{2,1,0:T(8,128)(2,1)} %bitcast.152), calls=%async_computation.4 | async-start | bytes 8388608 | tf_op jit(solution)/shard_map/all_to_all | solution.py:167
  467.4 15.6 %copy-start.1 = (bf16[256,256]{1,0:T(8,128)(2,1)S(1)}, bf16[256,256]{1,0:T(8,128)(2,1)}, u32[]{:S(2)}) copy-start(bf16[256,256]{1,0:T(8,128)(2,1)} %param.23) | copy-start | bytes 393220
Sparse Core Ops, SparseCore 0:
  8.9 19.4 all-gather.5
  30.5 57.7 all-gather.3
  90.4 131.3 all-gather.7
where the time goes:
time: 490 us
  waiting for transfers between devices  154 us (31%)
  blocking collectives  151 us (31%)
  matrix products  80.1 us (16%)
  local copies, waits for them, and re-layouts  40 us (8%)
  other arithmetic  30.5 us (6%)
  starting transfers between devices  17.9 us (4%)
  between operations  13.5 us (3%)
    all_to_all x1, blocking collectives, shards(): lax.all_to_all(outgoing, 'sp', split_axis=0, concat_axis=0, tiled=True)  95.5 us
    all_to_all x1, waiting for transfers between devices, shards(): lax.all_to_all(result.reshape(senders, slots_now, width), 'sp', split_axi...  91 us
    all_gather x1, blocking collectives, shards(): lax.all_gather(key_turned, 'sp', axis=0, tiled=True)  55.9 us
    dot_general x4, matrix products, one_block(): jnp.einsum('hbs,shd->bhd', attend, value_heads, preferred_element_type=jn...  36.8 us
    all_to_all x1, waiting for transfers between devices, shards(): lax.all_to_all(attended, 'sp', split_axis=0, concat_axis=1, tiled=True)  28 us
    all_to_all x1, waiting for transfers between devices, shards(): lax.all_to_all(query_turned, 'sp', split_axis=1, concat_axis=0, tiled=True)  17.7 us
    all_gather x1, waiting for transfers between devices, shards(): head_rows = lax.all_gather(out_proj, 'dp', axis=1, tiled=True)  16.1 us
    gather x2, local copies, waits for them, and re-layouts, combine_slots(): jnp.take(flat_back, slot_ids, axis=0).astype(jnp.float32)  12.4 us
  transfers between devices with their start and end apart: 7, of which 4 were waited for; matrix products, arithmetic and copies ran while one was open for 18% of the time, Pallas kernels for 0%

commit v1 on v0

--- a/solution.py
+++ b/solution.py
@@ -141,7 +141,10 @@
         ),
     )
     attended = attended.reshape(length, heads_here, -1)
-    token_heads = lax.all_to_all(attended, "sp", split_axis=0, concat_axis=1, tiled=True)
+    token_heads = jnp.concatenate(
+        lax.all_to_all(jnp.stack(jnp.split(attended, lax.axis_size("sp"), axis=0)), "sp", 0, 0),
+        axis=1,
+    )
     flat_heads = token_heads.reshape(tokens_here, -1)
     head_rows = lax.all_gather(out_proj, "dp", axis=1, tiled=True)
     projected = jnp.dot(

time: 490 us -> 483 us (0.986)
  waiting for transfers between devices: 154 us -> 136 us
  local copies, waits for them, and re-layouts: 40 us -> 49.2 us
    all_gather x1, waiting for transfers between devices: 16.1 us -> 0.02 us  [shards(): head_rows = lax.all_gather(out_proj, 'dp', axis=1, tiled=True)]
    unnamed x25 -> x32, local copies, waits for them, and re-layouts: 6.3 us -> 17.3 us
  transfers between devices with their start and end apart: 7 -> 7, of which waited for: 4 -> 3; matrix products, arithmetic and copies ran while one was open for 18% -> 20% of each run, Pallas kernels for 0% -> 0%
where the time goes in v1:
time: 483 us; the launch traced here: 482 us
  blocking collectives  150 us (31%)
  waiting for transfers between devices  136 us (28%)
  matrix products  80.3 us (17%)
  local copies, waits for them, and re-layouts  49.2 us (10%)
  other arithmetic  30.5 us (6%)
  starting transfers between devices  20 us (4%)
  between operations  13.5 us (3%)
    all_to_all x1, blocking collectives, shards(): lax.all_to_all(outgoing, 'sp', split_axis=0, concat_axis=0, tiled=True)  95.8 us
    all_to_all x1, waiting for transfers between devices, shards(): lax.all_to_all(result.reshape(senders, slots_now, width), 'sp', split_axi...  91.2 us
    all_gather x1, blocking collectives, shards(): lax.all_gather(key_turned, 'sp', axis=0, tiled=True)  54.6 us
    dot_general x4, matrix products, one_block(): jnp.einsum('hbs,shd->bhd', attend, value_heads, preferred_element_type=jn...  37 us
    all_to_all x1, waiting for transfers between devices, shards(): lax.all_to_all(jnp.stack(jnp.split(attended, lax.axis_size('sp'), axis=0)...  29.8 us
    unnamed x32, local copies, waits for them, and re-layouts  17.3 us
    all_to_all x1, waiting for transfers between devices, shards(): lax.all_to_all(query_turned, 'sp', split_axis=1, concat_axis=0, tiled=True)  13.1 us
    gather x2, local copies, waits for them, and re-layouts, combine_slots(): jnp.take(flat_back, slot_ids, axis=0).astype(jnp.float32)  12.4 us
  transfers between devices with their start and end apart: 7, of which 3 were waited for; matrix products, arithmetic and copies ran while one was open for 20% of the time, Pallas kernels for 0%

profile of v1, /device:TPU:0, one launch (start us, length us, event | category | flops | bytes accessed | tf_op | source)
XLA Modules:
  0.0 481.9 jit_solution(244415746128325746)
XLA Ops:
  8.3 1.7 fusion.35
  13.2 7.3 %all-to-all-start.1 = ((bf16[256,16,64]{0,2,1:T(8,128)(2,1)}), bf16[256,16,64]{0,2,1:T(8,128)(2,1)S(1)}, u32[]{:S(2)}, u32[]{:S(2)}) async-start(bf16[256,16,64]{0,2,1:T(8,128)(2,1)} %pad_maximum_fusion), calls=%async_computation.1 | async-start | bytes 1048576 | tf_op jit(solution)/shard_map/all_to_all | solution.py:100
  21.8 13.1 %all-to-all-done.1 = bf16[256,16,64]{0,2,1:T(8,128)(2,1)S(1)} async-done(((bf16[256,16,64]{0,2,1:T(8,128)(2,1)}), bf16[256,16,64]{0,2,1:T(8,128)(2,1)S(1)}, u32[]{:S(2)}, u32[]{:S(2)}) %all-to-all-start.1) | async-done | bytes 524320 | tf_op jit(solution)/shard_map/all_to_all | solution.py:100
  35.0 3.6 all-to-all-start
  39.4 54.6 %all_gather.13 = bf16[2048,64]{0,1:T(8,128)(2,1)S(1)} all-gather(bf16[256,64]{0,1:T(8,128)(2,1)S(1)} %pad_maximum_fusion.1), channel_id=1, replica_groups=mesh['sp'=8,'dp'=4] {'sp'}, dimensions={0}, use_global_device_ids=true | all-gather | bytes 294912 | tf_op jit(solution)/shard_map/all_gather | solution.py:96
  95.5 2.8 convolution_convert_fusion.1
  99.9 2.4 convolution_convert_fusion
  102.2 2.3 copy.63
  104.6 73.8 %while.11 = (s32[]{:T(128)}, bf16[4,512,2,128]{3,1,0,2:T(8,128)(2,1)}, s32[4]{0:T(128)S(1)}, bf16[4,512,2,128]{3,1,0,2:T(8,128)(2,1)S(1)}, bf16[2048,2,128]{2,0,...) while((s32[]{:T(128)}, ...), condition=%wide.region_4.5_spmd.clone, body=%wide.region_1.4_spmd.clone.sunk | while | flops 1360139776 | bytes 93205688 | solution.py:135
  107.7 2.8 fusion.83
  113.7 9.2 %fusion.85 = bf16[4,512,2,128]{3,1,0,2:T(8,128)(2,1)} fusion(bf16[4,512,2,128]{3,1,0,2:T(8,128)(2,1)} %get-tuple-element.195, s32[]{:T(128)} %get-tuple-element.194, bf16[2048,2,128]{2,0,1:T(8,128)(2,1)S(1)} %copy-done.5, f32[2,512]{1,0:T(2,128)S(1)} %fusion.84, f32[2,512,2048]{2,1,0:T(8,128)} %copy-done.2), kind=kOutput, calls=%fused_computation.13.clone.1 | convolution fusion | flops 543296512 | bytes 18092544 | tf_op jit(solution)/shard_map/while/body/eval_jaxpr/hbs,shd->bhd/dot_general | solution.py:131
  125.9 2.8 fusion.83
  130.3 2.1 copy-done.2
  132.4 9.6 %fusion.85 = bf16[4,512,2,128]{3,1,0,2:T(8,128)(2,1)} fusion(bf16[4,512,2,128]{3,1,0,2:T(8,128)(2,1)} %get-tuple-element.195, s32[]{:T(128)} %get-tuple-element.194, bf16[2048,2,128]{2,0,1:T(8,128)(2,1)S(1)} %copy-done.5, f32[2,512]{1,0:T(2,128)S(1)} %fusion.84, f32[2,512,2048]{2,1,0:T(8,128)} %copy-done.2), kind=kOutput, calls=%fused_computation.13.clone.1 | convolution fusion | flops 543296512 | bytes 18092544 | tf_op jit(solution)/shard_map/while/body/eval_jaxpr/hbs,shd->bhd/dot_general | solution.py:131
  145.1 2.8 fusion.83
  151.1 9.1 %fusion.85 = bf16[4,512,2,128]{3,1,0,2:T(8,128)(2,1)} fusion(bf16[4,512,2,128]{3,1,0,2:T(8,128)(2,1)} %get-tuple-element.195, s32[]{:T(128)} %get-tuple-element.194, bf16[2048,2,128]{2,0,1:T(8,128)(2,1)S(1)} %copy-done.5, f32[2,512]{1,0:T(2,128)S(1)} %fusion.84, f32[2,512,2048]{2,1,0:T(8,128)} %copy-done.2), kind=kOutput, calls=%fused_computation.13.clone.1 | convolution fusion | flops 543296512 | bytes 18092544 | tf_op jit(solution)/shard_map/while/body/eval_jaxpr/hbs,shd->bhd/dot_general | solution.py:131
  163.3 2.8 fusion.83
  169.3 9.1 %fusion.85 = bf16[4,512,2,128]{3,1,0,2:T(8,128)(2,1)} fusion(bf16[4,512,2,128]{3,1,0,2:T(8,128)(2,1)} %get-tuple-element.195, s32[]{:T(128)} %get-tuple-element.194, bf16[2048,2,128]{2,0,1:T(8,128)(2,1)S(1)} %copy-done.5, f32[2,512]{1,0:T(2,128)S(1)} %fusion.84, f32[2,512,2048]{2,1,0:T(8,128)} %copy-done.2), kind=kOutput, calls=%fused_computation.13.clone.1 | convolution fusion | flops 543296512 | bytes 18092544 | tf_op jit(solution)/shard_map/while/body/eval_jaxpr/hbs,shd->bhd/dot_general | solution.py:131
  191.0 4.1 all-to-all-start.2
  197.7 29.8 %all-to-all-done.2 = bf16[8,256,2,128]{3,1,2,0:T(8,128)(2,1)S(1)} async-done(((bf16[8,256,2,128]{3,1,2,0:T(8,128)(2,1)}), bf16[8,256,2,128]{3,1,2,0:T(8,128)(2,1)S(1)}, u32[]{:S(2)}, u32[]{:S(2)}) %all-to-all-start.2) | async-done | bytes 1048608 | tf_op jit(solution)/shard_map/all_to_all | solution.py:145
  228.1 6.1 %multiply_reduce_fusion.1 = (f32[256]{0:T(256)S(1)}, f32[256,2048]{1,0:T(8,128)S(1)}) fusion(bf16[256,2048]{0,1:T(8,128)(2,1)S(1)} %bitcast.180, bf16[2048,2048]{1,0:T(8,128)(2,1)} %all-gather.8.cloned.1.call-done, bf16[1,256,2048]{2,1,0:T(8,128)(2,1)} %param.21), kind=kOutput, calls=%fused_computation.42 | convolution fusion | flops 2150629120 | bytes 12583936 | tf_op jit(solution)/shard_map/dot_general | solution.py:150
  234.4 6.0 %gather_fusion = bf16[1024,2048]{1,0:T(8,128)(2,1)} fusion(bf16[256,2048]{1,0:T(8,128)(2,1)S(1)} %multiply_convert_fusion.1, s32[1024]{0:T(1024)S(1)} %broadcast_clamp_fusion), kind=kCustom, calls=%fused_computation | custom fusion | bytes 8392704 | tf_op jit(solution)/shard_map/jit(_take)/gather | solution.py:55
  240.4 2.6 select_select_fusion
  243.0 95.8 %all_to_all.45 = bf16[8,128,2048]{2,1,0:T(8,128)(2,1)S(1)} all-to-all(bf16[8,128,2048]{2,1,0:T(8,128)(2,1)S(1)} %select_select_fusion), channel_id=1, replica_groups=mesh['sp'=8,'dp'=4] {'sp'}, dimensions={0} | all-to-all | bytes 8388608 | tf_op jit(solution)/shard_map/all_to_all | solution.py:161
  338.8 4.5 fusion.20
  343.3 5.4 %multiply_convert_fusion = bf16[1024,1024]{1,0:T(8,128)(2,1)S(1)} fusion(f32[1024,1024]{1,0:T(8,128)S(1)} %fusion.20, bf16[1024,2048]{1,0:T(8,128)(2,1)S(1)} %bitcast.184, bf16[1,2048,1024]{2,1,0:T(8,128)(2,1)S(1)} %copy-done.10), kind=kOutput, calls=%fused_computation.31 | convolution fusion | flops 4301258752 | bytes 14680064 | tf_op jit(solution)/shard_map/dot_general | solution.py:164
  348.7 6.1 %fusion.24 = bf16[1024,2048]{1,0:T(8,128)(2,1)} fusion(bf16[1024,1024]{1,0:T(8,128)(2,1)S(1)} %multiply_convert_fusion, bf16[1,1024,2048]{2,1,0:T(8,128)(2,1)S(1)} %copy-done.11), kind=kOutput, calls=%fused_computation.34 | convolution fusion | flops 4297064448 | bytes 10485760 | tf_op jit(solution)/shard_map/dot_general | solution.py:167
  354.7 4.9 %all-to-all-start.4 = ((bf16[8,128,2048]{2,1,0:T(8,128)(2,1)}), bf16[8,128,2048]{2,1,0:T(8,128)(2,1)}, u32[]{:S(2)}, u32[]{:S(2)}) async-start(bf16[8,128,2048]{2,1,0:T(8,128)(2,1)} %bitcast.182), calls=%async_computation.4 | async-start | bytes 8388608 | tf_op jit(solution)/shard_map/all_to_all | solution.py:170
  360.6 91.2 %all-to-all-done.4 = bf16[8,128,2048]{2,1,0:T(8,128)(2,1)} async-done(((bf16[8,128,2048]{2,1,0:T(8,128)(2,1)}), bf16[8,128,2048]{2,1,0:T(8,128)(2,1)}, u32[]{:S(2)}, u32[]{:S(2)}) %all-to-all-start.4) | async-done | bytes 4194336 | tf_op jit(solution)/shard_map/all_to_all | solution.py:170
  451.8 8.0 %gather_fusion.1 = bf16[512,2048]{1,0:T(8,128)(2,1)} fusion(bf16[1024,2048]{1,0:T(8,128)(2,1)} %bitcast.40, s32[1024]{0:T(1024)S(1)} %pad_clamp_fusion), kind=kCustom, calls=%fused_computation.1 | custom fusion | bytes 4196352 | tf_op jit(solution)/shard_map/jit(_take)/gather | solution.py:63
  459.8 4.4 gather.15
  464.2 9.9 %multiply_reduce_fusion = f32[256,2048]{1,0:T(8,128)S(1)} fusion(bf16[256,2,2048]{2,1,0:T(2,128)(2,1)} %gather.15, pred[256,2]{1,0:T(8,128)(4,1)S(1)} %copy.70, f32[256,2]{1,0:T(8,128)S(1)} %copy.66), kind=kLoop, calls=%fused_computation.30 | loop fusion | flops 3670016 | bytes 4196864 | tf_op jit(solution)/shard_map/reduce_sum | solution.py:65
  (120 shorter events, 49.2 us)
Async XLA Ops:
  6.5 88.9 %copy-start = (bf16[256,256]{1,0:T(8,128)(2,1)S(1)}, bf16[256,256]{1,0:T(8,128)(2,1)}, u32[]{:S(2)}) copy-start(bf16[256,256]{1,0:T(8,128)(2,1)} %param.23) | copy-start | bytes 393220
  6.5 13.9 %copy-start.4 = (bf16[1,256,16,128]{3,2,1,0:T(8,128)(2,1)S(1)}, bf16[1,256,16,128]{3,2,1,0:T(8,128)(2,1)}, u32[]{:S(2)}) copy-start(bf16[1,256,16,128]{3,2,1,0:T(8,128)(2,1)} %param.17) | copy-start | bytes 3145732
  6.5 32.1 %all-gather.6.cloned.1.call-start = ((), (), s32[]{:S(2)}) async-start(), calls=%async_computation.6 | async-start | bytes 1310720 | tf_op jit(solution)/shard_map/all_gather | solution.py:149
  7.3 88.2 %all-gather.4.cloned.1.call-start = ((), (), s32[]{:S(2)}) async-start(), calls=%async_computation.5 | async-start | bytes 1179648 | tf_op jit(solution)/shard_map/all_gather | solution.py:95
  13.2 21.8 %all-to-all-start.1 = ((bf16[256,16,64]{0,2,1:T(8,128)(2,1)}), bf16[256,16,64]{0,2,1:T(8,128)(2,1)S(1)}, u32[]{:S(2)}, u32[]{:S(2)}) async-start(bf16[256,16,64]{0,2,1:T(8,128)(2,1)} %pad_maximum_fusion), calls=%async_computation.1 | async-start | bytes 1048576 | tf_op jit(solution)/shard_map/all_to_all | solution.py:100
  35.0 69.6 %all-to-all-start = ((bf16[256,16,128]{2,0,1:T(8,128)(2,1)}), bf16[256,16,128]{2,0,1:T(8,128)(2,1)S(1)}, u32[]{:S(2)}, u32[]{:S(2)}) async-start(bf16[256,16,128]{2,0,1:T(8,128)(2,1)} %bitcast.157), calls=%async_computation | async-start | bytes 2097152 | tf_op jit(solution)/shard_map/all_to_all | solution.py:99
  38.6 189.4 %all-gather.8.cloned.1.call-start = ((), (), s32[]{:S(2)}) async-start(), calls=%async_computation.7 | async-start | bytes 9437184 | tf_op jit(solution)/shard_map/all_gather | solution.py:152
  95.5 4.4 copy-start.3
  110.5 3.2 copy-start.2
  110.5 3.2 copy-start.5
  128.7 3.7 copy-start.2
  128.8 3.7 copy-start.5
  147.9 3.2 copy-start.2
  147.9 3.2 copy-start.5
  166.1 3.2 copy-start.2
  166.1 3.2 copy-start.5
  178.4 16.6 %copy-start.6 = (s32[1,256,2]{1,2,0:T(2,128)S(1)}, s32[1,256,2]{1,2,0:T(2,128)}, u32[]{:S(2)}) copy-start(s32[1,256,2]{1,2,0:T(2,128)} %param.30) | copy-start | bytes 6148
  191.0 36.5 %all-to-all-start.2 = ((bf16[8,256,2,128]{3,1,2,0:T(8,128)(2,1)}), bf16[8,256,2,128]{3,1,2,0:T(8,128)(2,1)S(1)}, u32[]{:S(2)}, u32[]{:S(2)}) async-start(bf16[8,256,2,128]{3,1,2,0:T(8,128)(2,1)} %fusion.36), calls=%async_computation.2 | async-start | bytes 2097152 | tf_op jit(solution)/shard_map/all_to_all | solution.py:145
  228.1 6.1 %copy-start.7 = (f32[2048]{0:T(1024)S(1)}, f32[2048]{0:T(1024)}, u32[]{:S(2)}) copy-start(f32[2048]{0:T(1024)} %param.26) | copy-start | bytes 24580
  243.0 95.8 %copy-start.9 = (bf16[1,2048,1024]{2,1,0:T(8,128)(2,1)S(1)}, bf16[1,2048,1024]{2,1,0:T(8,128)(2,1)}, u32[]{:S(2)}) copy-start(bf16[1,2048,1024]{2,1,0:T(8,128)(2,1)} %param.28) | copy-start | bytes 12582916
  338.8 4.5 copy-start.10
  343.3 5.4 %copy-start.11 = (bf16[1,1024,2048]{2,1,0:T(8,128)(2,1)S(1)}, bf16[1,1024,2048]{2,1,0:T(8,128)(2,1)}, u32[]{:S(2)}) copy-start(bf16[1,1024,2048]{2,1,0:T(8,128)(2,1)} %param.29) | copy-start | bytes 12582916
  354.7 5.6 %copy-start.8 = (f32[1,256,2]{1,2,0:T(2,128)S(1)}, f32[1,256,2]{1,2,0:T(2,128)}, u32[]{:S(2)}) copy-start(f32[1,256,2]{1,2,0:T(2,128)} %param.31) | copy-start | bytes 6148
  354.7 97.0 %all-to-all-start.4 = ((bf16[8,128,2048]{2,1,0:T(8,128)(2,1)}), bf16[8,128,2048]{2,1,0:T(8,128)(2,1)}, u32[]{:S(2)}, u32[]{:S(2)}) async-start(bf16[8,128,2048]{2,1,0:T(8,128)(2,1)} %bitcast.182), calls=%async_computation.4 | async-start | bytes 8388608 | tf_op jit(solution)/shard_map/all_to_all | solution.py:170
  459.7 15.6 %copy-start.1 = (bf16[256,256]{1,0:T(8,128)(2,1)S(1)}, bf16[256,256]{1,0:T(8,128)(2,1)}, u32[]{:S(2)}) copy-start(bf16[256,256]{1,0:T(8,128)(2,1)} %param.23) | copy-start | bytes 393220
Sparse Core Ops, SparseCore 0:
  8.9 19.4 all-gather.5
  30.5 49.5 all-gather.3
  82.2 132.9 all-gather.7
